TPU v7x, 32 devices: a whole 2x2x4 slice. The times are simulated.
32 devices in a mesh: sp: 8 (over z, y), fs: 2 (over x), tp: 2 (over core).
Axes of the slice: x: 2, y: 2, z: 4, core: 2. Of those that a mesh axis runs over, the one named last changes fastest.
Arguments:
- ret_query: bfloat16 [1024, 2, 512], P('sp', 'fs', 'tp'), may hold values from -6 to 6
- ret_key: bfloat16 [1024, 2, 512], P('sp', 'fs', 'tp'), may hold values from -6 to 6
- ret_value: bfloat16 [1024, 2, 1024], P('sp', 'fs', 'tp'), may hold values from -6 to 6
- log_decay: float32 [2, 4, 1024], P('fs', 'tp', 'sp'), may hold values from -1.2 to 0
- ret_gain: float32 [1024], P('tp'), may hold values from 0.1 to 1.9
- mla_query: bfloat16 [1024, 2, 1536], P('sp', 'fs', 'tp'), may hold values from -64 to 64
- kv_latent: bfloat16 [1024, 2, 256], P('sp', 'fs'), may hold values from -6 to 6
- rope_key: bfloat16 [1024, 2, 64], P('sp', 'fs'), may hold values from -8 to 8
- key_up: bfloat16 [256, 1024], replicated, may hold values from -0.375 to 0.375
- value_up: bfloat16 [256, 1024], replicated, may hold values from -3 to 3
- ret_out: bfloat16 [1024, 2048], P('tp', 'fs'), may hold values from -0.1875 to 0.1875
- mla_out: bfloat16 [1024, 2048], P('tp', 'fs'), may hold values from -0.1875 to 0.1875
Outputs:
- mixed_rows: bfloat16 [1024, 2, 2048], P(('sp', 'tp'), 'fs')
- log_weight: float32 [2, 8, 1024], P('fs', 'tp', 'sp')
All inputs are finite; a program needn't handle non-finite values.
Results may differ from a plain program's by a relative error of at most 0.014.
Values may be sent and summed in bfloat16 or wider, within the bound.
A program may use at most 128 MiB of HBM per device.

v0:
```python
import jax
import jax.numpy as jnp
from jax import lax
from jax.sharding import PartitionSpec as P

QK = 128
VD = 256
NOPE = 128
ROPE = 64
VDM = 128
KVR = 256


def entering(x, axis, join, neutral):
    place = lax.axis_index(axis)
    gathered = jax.tree.map(
        lambda a, kind: lax.all_gather(a.astype(kind), axis), x, (jnp.bfloat16, jnp.bfloat16)
    )
    state = jax.tree.map(lambda a, e: jnp.zeros_like(a) + jnp.asarray(e, a.dtype), x, neutral)

    def one(lap, state):
        return join(
            state,
            jax.tree.map(
                lambda a, own: lax.dynamic_index_in_dim(a, lap, 0, False).astype(own.dtype),
                gathered,
                x,
            ),
        )

    return lax.fori_loop(0, place, one, state)


def rotate(vectors, positions):
    half_width = vectors.shape[-1] // 2
    inverse = 1.0 / 10000.0 ** (jnp.arange(half_width, dtype=jnp.float32) / half_width)
    angles = positions.astype(jnp.float32)[:, None] * inverse[None, :]
    cosine = jnp.cos(angles)[:, None, None, :]
    sine_part = jnp.sin(angles)[:, None, None, :]
    widened = vectors.astype(jnp.float32)
    front_part = widened[..., :half_width]
    back_part = widened[..., half_width:]
    turned = jnp.concatenate(
        [front_part * cosine - back_part * sine_part, front_part * sine_part + back_part * cosine],
        axis=-1,
    )
    return turned.astype(jnp.bfloat16)


def chain_step(earlier, later):
    return (earlier[0] * later[0], later[0][..., None, None] * earlier[1] + later[1])


def on_device(
    ret_query,
    ret_key,
    ret_value,
    log_decay,
    ret_gain,
    mla_query,
    kv_latent,
    rope_key,
    key_up,
    value_up,
    ret_out,
    mla_out,
):
    span_rows = ret_query.shape[0]
    groups = ret_query.shape[1]
    ret_local = ret_value.shape[2] // VD
    mla_local = mla_query.shape[2] // (NOPE + ROPE)
    core_index = lax.axis_index("tp")
    offset = lax.axis_index("sp") * span_rows
    positions = offset + jnp.arange(span_rows, dtype=jnp.int32)
    queries = rotate(ret_query.reshape(span_rows, groups, ret_local, QK), positions)
    key_rows = rotate(ret_key.reshape(span_rows, groups, ret_local, QK), positions)
    value_rows = ret_value.reshape(span_rows, groups, ret_local, VD)
    logit_scale = QK ** (-0.5)
    cumulative = jnp.cumsum(log_decay, axis=-1)
    log_gap = cumulative[..., :, None] - cumulative[..., None, :]
    causal = jnp.tril(jnp.ones((span_rows, span_rows), dtype=bool))
    score_matrix = (
        jnp.einsum("ishd,jshd->shij", queries, key_rows, preferred_element_type=jnp.float32)
        * logit_scale
    )
    weights = jnp.where(
        causal, score_matrix * jnp.exp(jnp.where(causal, log_gap, 0.0)), 0.0
    ).astype(jnp.bfloat16)
    intra_block = jnp.einsum(
        "shij,jshe->ishe", weights, value_rows, preferred_element_type=jnp.float32
    )
    tail_decay = jnp.transpose(jnp.exp(cumulative[..., -1:] - cumulative), (2, 0, 1))[..., None]
    block_state = jnp.einsum(
        "jshd,jshe->shde",
        key_rows.astype(jnp.float32) * tail_decay,
        value_rows.astype(jnp.float32),
        precision=lax.Precision.HIGHEST,
    )
    block_decay = jnp.exp(cumulative[..., -1])
    _, carried = entering(
        (block_decay, block_state),
        "sp",
        chain_step,
        (jnp.ones_like(block_decay), jnp.zeros_like(block_state)),
    )
    growth = jnp.transpose(jnp.exp(cumulative), (2, 0, 1))[..., None]
    cross_term = (
        jnp.einsum(
            "ishd,shde->ishe", queries.astype(jnp.float32), carried, precision=lax.Precision.HIGHEST
        )
        * logit_scale
        * growth
    )
    retained = intra_block + cross_term
    normed = (
        retained
        * lax.rsqrt(jnp.mean(retained * retained, axis=-1, keepdims=True) + 1e-06)
        * ret_gain.reshape(ret_local, VD)
    )
    ret_heads = normed.astype(jnp.bfloat16).reshape(span_rows, groups, ret_local * VD)
    head_rows = mla_query.reshape(span_rows, groups, mla_local, NOPE + ROPE)
    query_rope = rotate(head_rows[..., NOPE:], positions)
    up_keys = lax.dynamic_slice_in_dim(
        key_up, core_index * (mla_local * NOPE), mla_local * NOPE, 1
    ).reshape(KVR, mla_local, NOPE)
    absorbed = jnp.einsum(
        "bghn,chn->bghc", head_rows[..., :NOPE], up_keys, preferred_element_type=jnp.float32
    ).astype(jnp.bfloat16)
    own_rope = rotate(rope_key[:, :, None, :], positions)[:, :, 0, :]
    joined = jnp.concatenate([kv_latent, own_rope], axis=-1)
    attn_scale = (NOPE + ROPE) ** (-0.5)
    last_position = offset + span_rows - 1
    initial = (
        jnp.full((groups, mla_local, span_rows), -jnp.inf, jnp.float32),
        jnp.zeros((groups, mla_local, span_rows), jnp.float32),
        jnp.zeros((groups, mla_local, span_rows, KVR), jnp.float32),
    )
    piece = lax.all_gather(joined, "sp", axis=0, tiled=True)

    def compute(current):
        row_max, total, weighted = current
        latent = piece[..., :KVR]
        rotated = piece[..., KVR:]
        key_count = piece.shape[0]
        block_scores = (
            jnp.einsum("bghc,pgc->ghbp", absorbed, latent, preferred_element_type=jnp.float32)
            + jnp.einsum("bghr,pgr->ghbp", query_rope, rotated, preferred_element_type=jnp.float32)
        ) * attn_scale
        key_positions = jnp.arange(key_count, dtype=jnp.int32)
        visible = key_positions[None, :] <= positions[:, None]
        block_scores = jnp.where(visible, block_scores, -jnp.inf)
        new_max = jnp.max(block_scores, axis=-1)
        safe_max = jnp.where(new_max == -jnp.inf, 0.0, new_max)
        exponent = jnp.exp(block_scores - safe_max[..., None])
        rescale = jnp.exp(row_max - safe_max)
        total = total * rescale + jnp.sum(exponent, axis=-1)
        weighted = weighted * rescale[..., None] + jnp.einsum(
            "ghbp,pgc->ghbc",
            exponent.astype(jnp.bfloat16),
            latent,
            preferred_element_type=jnp.float32,
        )
        return (new_max, total, weighted)

    def unchanged(current):
        return current

    row_max, total, weighted = lax.cond(jnp.int32(0) <= last_position, compute, unchanged, initial)
    log_weight = row_max + jnp.log(total)
    latent_mean = (weighted / total[..., None]).astype(jnp.bfloat16)
    up_values = lax.dynamic_slice_in_dim(
        value_up, core_index * (mla_local * VDM), mla_local * VDM, 1
    ).reshape(KVR, mla_local, VDM)
    mla_heads = (
        jnp.einsum("ghbc,chv->bghv", latent_mean, up_values, preferred_element_type=jnp.float32)
        .astype(jnp.bfloat16)
        .reshape(span_rows, groups, mla_local * VDM)
    )
    ret_matrix, mla_matrix = (ret_out, mla_out)
    ret_source, mla_source = (
        lax.all_gather(ret_heads, "fs", axis=1, tiled=True),
        lax.all_gather(mla_heads, "fs", axis=1, tiled=True),
    )
    mixed_rows = lax.psum_scatter(
        (
            jnp.einsum("bgk,kd->bgd", ret_source, ret_matrix, preferred_element_type=jnp.float32)
            + jnp.einsum("bgk,kd->bgd", mla_source, mla_matrix, preferred_element_type=jnp.float32)
        ).astype(jnp.bfloat16),
        "tp",
        scatter_dimension=0,
        tiled=True,
    )
    mixed_rows = lax.all_to_all(mixed_rows, "fs", split_axis=1, concat_axis=2, tiled=True)
    return (mixed_rows, log_weight)


def solution(mesh):
    in_specs = (
        P("sp", "fs", "tp"),
        P("sp", "fs", "tp"),
        P("sp", "fs", "tp"),
        P("fs", "tp", "sp"),
        P("tp"),
        P("sp", "fs", "tp"),
        P("sp", "fs", None),
        P("sp", "fs", None),
        P(),
        P(),
        P("tp", "fs"),
        P("tp", "fs"),
    )
    out_specs = (P(("sp", "tp"), "fs", None), P("fs", "tp", "sp"))
    return jax.shard_map(
        on_device, mesh=mesh, in_specs=in_specs, out_specs=out_specs, check_vma=False
    )
```

profile of v0, /device:TPU:0, one launch (start us, length us, event | category | flops | bytes accessed | tf_op | source)
XLA Modules:
  0.0 123.5 jit_solution(4791576793776941514)
XLA Ops:
  7.2 0.0 copy-start
  7.2 0.0 copy-start.3
  7.2 0.0 copy-start.6
  7.2 0.0 copy-start.4
  7.2 0.0 all-gather.4.cloned.1.call-start
  7.3 1.1 copy.85
  8.4 0.1 copy.117
  8.5 0.1 copy.118
  8.6 1.0 copy.88
  9.6 0.1 copy.119
  9.7 0.1 copy.120
  9.8 1.0 reduce_window_sum.11
  10.8 0.2 slice_reduce_fusion
  11.0 0.1 multiply_bitcast_fusion
  11.0 1.0 reshape.580
  12.0 0.3 multiply_cosine_fusion
  12.3 0.1 fusion.36
  12.4 1.1 convolution_convert_fusion.2
  13.5 0.0 all-gather.4.cloned.1.call-update
  13.5 0.0 reduce-scatter.2.cloned.1.call-start
  13.6 0.0 copy-start.7
  13.6 0.2 copy.105
  13.8 0.1 fusion.55
  13.9 0.1 copy.102
  14.0 0.1 copy.103
  14.2 22.3 %all-gather = bf16[8,2,1]{2,1,0:T(2,128)(2,1)S(1)} all-gather(bf16[1,2,1]{2,1,0:T(2,128)(2,1)S(1)} %get-tuple-element.148), channel_id=2, replica_groups=mesh['sp'=8,'fs'=2,'tp'=2] {'sp'}, dimensions={0}, use_global_device_ids=true | all-gather | bytes 36 | tf_op jit(solution)/shard_map/all_gather | solution.py:17
  36.5 0.1 copy.121
  36.7 0.1 copy.101
  36.8 0.8 multiply_cosine_fusion.1
  37.7 0.9 pad_maximum_fusion
  38.6 0.3 fusion.18
  38.9 33.1 %all_gather.23 = bf16[1024,1,320]{2,0,1:T(8,128)(2,1)S(1)} all-gather(bf16[128,1,320]{2,0,1:T(8,128)(2,1)S(1)} %pad_maximum_fusion), channel_id=1, replica_groups=mesh['sp'=8,'fs'=2,'tp'=2] {'sp'}, dimensions={0}, use_global_device_ids=true | all-gather | bytes 737280 | tf_op jit(solution)/shard_map/all_gather | solution.py:138
  72.0 5.0 %conditional.1 = (f32[1,4,128]{2,1,0:T(4,128)}, f32[1,4,128]{2,1,0:T(4,128)S(1)}, f32[1,4,128,256]{3,2,1,0:T(8,128)S(1)}, f32[1,4,128]{2,1,0:T(4,128)S(1)}) conditional(s32[]{:T(128)} %convert_element_type.188, () %tuple.24, (s32[]{:T(128)}, s32[128]{0:T(128)S(1)}, bf16[1024,1,320]{2,0,1:T(8,128)(2,1)S(1)}, bf16[128,1,4,256]{0,3,2,1:T(8,128)(2,1)S(1)}, ...), branch_computations={%region_4.5_spmd, %region_5.8_spmd} | conditional | flops 608439936 | bytes 16213568 | solution.py:168
  72.0 0.3 copy.83
  72.3 0.5 fusion.11
  72.8 0.1 iota_compare_fusion
  72.9 1.1 fusion.64
  73.9 0.7 exponential_multiply_fusion
  74.6 1.3 %fusion.2 = f32[1,4,128,256]{3,2,1,0:T(8,128)} fusion(f32[1,4,128,1024]{2,3,1,0:T(8,128)S(1)} %get-tuple-element.126, f32[4,128]{1,0:T(4,128)S(1)} %get-tuple-element.124, bf16[1024,1,320]{2,0,1:T(8,128)(2,1)S(1)} %get-tuple-element.57, f32[4,128]{1,0:T(4,128)S(1)} %get-tuple-element.123), kind=kOutput, calls=%fused_computation.8 | convolution fusion | flops 269615104 | bytes 3149824 | tf_op jit(solution)/shard_map/cond/branch_1_fun/ghbp,pgc->ghbc/dot_general | solution.py:157
  76.0 0.3 fusion.1
  76.2 0.7 fusion.62
  76.9 0.1 copy-done.2
  77.0 0.3 convolution_convert_fusion.1
  77.3 0.1 copy.109
  77.4 0.1 copy.92
  77.5 0.1 copy-done.8
  77.7 5.6 %all_gather.24 = bf16[128,2,512]{2,0,1:T(8,128)(2,1)S(1)} all-gather(bf16[128,1,512]{2,0,1:T(8,128)(2,1)S(1)} %copy.109), channel_id=1, replica_groups=mesh['sp'=8,'fs'=2,'tp'=2] {'fs'}, dimensions={1}, use_global_device_ids=true | all-gather | bytes 393216 | tf_op jit(solution)/shard_map/all_gather | solution.py:182
  83.3 0.0 all-gather.4.cloned.1.call-done
  83.4 0.3 fusion.20
  83.7 0.0 copy-start.1
  83.7 0.5 multiply_reduce_fusion
  84.2 0.1 multiply_convert_fusion
  84.4 0.1 copy.99
  84.5 0.1 copy.100
  84.6 5.6 %all_gather.22 = bf16[128,2,512]{2,0,1:T(8,128)(2,1)S(1)} all-gather(bf16[128,1,512]{2,0,1:T(8,128)(2,1)S(1)} %copy.100), channel_id=1, replica_groups=mesh['sp'=8,'fs'=2,'tp'=2] {'fs'}, dimensions={1}, use_global_device_ids=true | all-gather | bytes 393216 | tf_op jit(solution)/shard_map/all_gather | solution.py:181
  90.2 0.5 fusion.25
  90.7 1.2 %fusion.17 = bf16[128,2,1024]{2,0,1:T(8,128)(2,1)} fusion(f32[128,2,1024]{2,0,1:T(8,128)S(1)} %fusion.25, bf16[128,2,512]{2,0,1:T(8,128)(2,1)S(1)} %all_gather.24, bf16[512,1024]{1,0:T(8,128)(2,1)S(1)} %copy-done.1), kind=kOutput, calls=%fused_computation.29 | convolution fusion | flops 268959744 | bytes 2883584 | tf_op jit(solution)/shard_map/bgk,kd->bgd/dot_general | solution.py:187
  92.0 0.0 reduce-scatter.2.cloned.1.call-update
  92.0 14.2 %reduce-scatter.2.cloned.1.call-done = bf16[64,2,1024]{2,0,1:T(8,128)(2,1)} async-done(((bf16[128,2,1024]{2,0,1:T(8,128)(2,1)}), bf16[64,2,1024]{2,0,1:T(8,128)(2,1)}) %reduce-scatter.2.cloned.1.call-update) | async-done | bytes 262160 | tf_op jit(solution)/shard_map/reduce_scatter | solution.py:184
  106.2 3.4 %all-to-all-start = ((bf16[64,2,1024]{2,0,1:T(8,128)(2,1)}), bf16[64,2,1024]{2,0,1:T(8,128)(2,1)S(1)}, u32[]{:S(2)}, u32[]{:S(2)}) async-start(bf16[64,2,1024]{2,0,1:T(8,128)(2,1)} %reduce-scatter.2.cloned.1.call-done), calls=%async_computation.1 | async-start | bytes 524288 | tf_op jit(solution)/shard_map/all_to_all | solution.py:193
  109.6 1.3 %add.106 = f32[1,4,128]{2,1,0:T(4,128)} add(f32[1,4,128]{2,1,0:T(4,128)} %get-tuple-element.69, f32[1,4,128]{2,1,0:T(4,128)S(1)} %get-tuple-element.110) | non-fusion elementwise | flops 512 | bytes 6144 | tf_op jit(solution)/shard_map/add | solution.py:169
  110.9 4.6 %all-to-all-done = bf16[64,2,1024]{2,0,1:T(8,128)(2,1)S(1)} async-done(((bf16[64,2,1024]{2,0,1:T(8,128)(2,1)}), bf16[64,2,1024]{2,0,1:T(8,128)(2,1)S(1)}, u32[]{:S(2)}, u32[]{:S(2)}) %all-to-all-start) | async-done | bytes 262176 | tf_op jit(solution)/shard_map/all_to_all | solution.py:193
  115.5 0.3 copy.110
  115.8 0.9 all_to_all.10
  (27 shorter events, 0.2 us)
Async XLA Ops:
  7.2 83.1 %copy-start = (bf16[512,1024]{1,0:T(8,128)(2,1)S(1)}, bf16[512,1024]{1,0:T(8,128)(2,1)}, u32[]{:S(2)}) copy-start(bf16[512,1024]{1,0:T(8,128)(2,1)} %param.26) | copy-start | bytes 3145732
  7.2 6.4 %copy-start.3 = (bf16[128,1,768]{2,0,1:T(8,128)(2,1)S(1)}, bf16[128,1,768]{2,0,1:T(8,128)(2,1)}, u32[]{:S(2)}) copy-start(bf16[128,1,768]{2,0,1:T(8,128)(2,1)} %param.21) | copy-start | bytes 589828
  7.2 6.5 %copy-start.6 = (bf16[128,1,64]{0,2,1:T(8,128)(2,1)S(1)}, bf16[128,1,64]{0,2,1:T(8,128)(2,1)}, u32[]{:S(2)}) copy-start(bf16[128,1,64]{0,2,1:T(8,128)(2,1)} %param.23) | copy-start | bytes 49156
  7.2 29.3 %copy-start.4 = (bf16[256,1024]{1,0:T(8,128)(2,1)S(1)}, bf16[256,1024]{1,0:T(8,128)(2,1)}, u32[]{:S(2)}) copy-start(bf16[256,1024]{1,0:T(8,128)(2,1)} %param.24) | copy-start | bytes 1572868
  7.2 29.3 %copy-start.5 = (bf16[256,1024]{1,0:T(8,128)(2,1)S(1)}, bf16[256,1024]{1,0:T(8,128)(2,1)}, u32[]{:S(2)}) copy-start(bf16[256,1024]{1,0:T(8,128)(2,1)} %param.25) | copy-start | bytes 1572868
  7.2 76.1 %all-gather.4.cloned.1.call-start = ((), (), s32[]{:S(2)}) async-start(), calls=%async_computation.3 | async-start | bytes 1179648 | tf_op jit(solution)/shard_map/all_gather | solution.py:17
  13.5 92.7 %reduce-scatter.2.cloned.1.call-start = ((), (), s32[]{:S(2)}) async-start(), calls=%async_computation.2 | async-start | bytes 786432 | tf_op jit(solution)/shard_map/reduce_scatter | solution.py:184
  13.6 0.6 copy-start.7
  75.9 1.0 copy-start.2
  77.0 0.7 copy-start.8
  83.7 7.0 %copy-start.1 = (bf16[512,1024]{1,0:T(8,128)(2,1)S(1)}, bf16[512,1024]{1,0:T(8,128)(2,1)}, u32[]{:S(2)}) copy-start(bf16[512,1024]{1,0:T(8,128)(2,1)} %param.27) | copy-start | bytes 3145732
  106.2 9.3 %all-to-all-start = ((bf16[64,2,1024]{2,0,1:T(8,128)(2,1)}), bf16[64,2,1024]{2,0,1:T(8,128)(2,1)S(1)}, u32[]{:S(2)}, u32[]{:S(2)}) async-start(bf16[64,2,1024]{2,0,1:T(8,128)(2,1)} %reduce-scatter.2.cloned.1.call-done), calls=%async_computation.1 | async-start | bytes 524288 | tf_op jit(solution)/shard_map/all_to_all | solution.py:193
Sparse Core Ops, SparseCore 0:
  13.6 46.8 all-gather.3
  92.1 14.0 reduce-scatter.1
where the time goes:
time: 124 us
  blocking collectives  66.7 us (54%)
  waiting for transfers between devices  18.9 us (15%)
  between operations  14.4 us (12%)
  matrix products  6.98 us (6%)
  other arithmetic  6.73 us (5%)
  local copies, waits for them, and re-layouts  6.26 us (5%)
  starting transfers between devices  3.52 us (3%)
    all_gather x1, blocking collectives, on_device(): piece = lax.all_gather(joined, 'sp', axis=0, tiled=True)  33.1 us
    all_gather x1, blocking collectives, entering(): lax.all_gather(a.astype(kind), axis)  22.3 us
    reduce_scatter x1, waiting for transfers between devices, on_device(): lax.psum_scatter((jnp.einsum('bgk,kd->bgd', ret_source, ret_matrix, prefe...  14.2 us
    all_gather x1, blocking collectives, on_device(): lax.all_gather(ret_heads, 'fs', axis=1, tiled=True)  5.64 us
    all_gather x1, blocking collectives, on_device(): lax.all_gather(mla_heads, 'fs', axis=1, tiled=True)  5.62 us
    all_to_all x1, waiting for transfers between devices, on_device(): lax.all_to_all(mixed_rows, 'fs', split_axis=1, concat_axis=2, tiled=True)  4.61 us
    all_to_all x1, starting transfers between devices, on_device(): lax.all_to_all(mixed_rows, 'fs', split_axis=1, concat_axis=2, tiled=True)  3.44 us
    unnamed x24, local copies, waits for them, and re-layouts  2.9 us
  transfers between devices with their start and end apart: 3, of which 2 were waited for; matrix products, arithmetic and copies ran while one was open for 8% of the time, Pallas kernels for 0%

commit v1 on v0

v1 whole, which is shorter than its diff:
```python
import functools
import math

import jax
import jax.numpy as jnp
import numpy as np
from jax import lax
from jax.experimental import pallas as pl
from jax.experimental.pallas import tpu as pltpu
from jax.sharding import PartitionSpec as P

QK = 128
VD = 256
NOPE = 128
ROPE = 64
VDM = 128
KVR = 256
KW = 384
MESH = pl.DeviceIdType.MESH
BF = jnp.bfloat16
F32 = jnp.float32


def tables(half, rows, places):
    inverse = 1.0 / 10000.0 ** (np.arange(half) / half)
    inverse = np.concatenate([inverse, inverse])
    near = np.arange(rows)[:, None] * inverse[None, :]
    far = (np.arange(places) * rows)[:, None] * inverse[None, :]
    swap = np.zeros((2 * half, 2 * half), np.float32)
    for j in range(half):
        swap[half + j, j] = -1.0
        swap[j, half + j] = 1.0
    return (
        np.stack([np.cos(near), np.sin(near)]).astype(np.float32),
        np.stack([np.cos(far), np.sin(far)]).astype(np.float32),
        swap,
    )


def dot(a, b):
    return jnp.dot(a, b, preferred_element_type=F32)


def dot_nt(a, b, precision=None):
    return lax.dot_general(
        a, b, (((1,), (1,)), ((), ())), precision=precision, preferred_element_type=F32
    )


def kernel(
    sizes,
    rq_ref, rk_ref, rv_ref, ld_ref, gain_ref, mq_ref, kv_ref, rope_ref,
    near_r, far_r, swap_r, near_m, far_m, swap_m,
    ku_hbm, vu_hbm, ro_hbm, mo_hbm,
    out_ref, lw_ref,
    ku, vu, ro, mo,
    kvb, q_ref, m_ref, l_ref, acc_ref,
    dec_own, dec, st_own, st_in, pre_out, pre_in,
    gath, part, tin, osum, oin, intra_ref, rot_ref, grow_ref,
    w_sem, d_send, d_recv, s_send, s_recv, h_send, h_recv, k_send, k_recv,
    f_send, f_recv, g_send, g_recv, t_send, t_recv, o_send, o_recv,
):
    NP, NF, NT, RL, ML, G = sizes
    stride = NP // G
    rows = rq_ref.shape[0]
    half = rows // NT
    r = st_own.shape[1]
    me = lax.axis_index("sp")
    fs = lax.axis_index("fs")
    tp = lax.axis_index("tp")

    def remote(src, dst, ss, rs, axis, to):
        return pltpu.make_async_remote_copy(
            src_ref=src, dst_ref=dst, send_sem=ss, recv_sem=rs,
            device_id={axis: to}, device_id_type=MESH,
        )

    barrier = pltpu.get_barrier_semaphore()
    for axis, count, own in (("sp", NP, me), ("fs", NF, fs), ("tp", NT, tp)):
        for k in range(1, count):
            pl.semaphore_signal(
                barrier, inc=1, device_id={axis: lax.rem(own + k, count)}, device_id_type=MESH
            )

    wk, wv = ML * NOPE, ML * VDM
    weights = [
        pltpu.make_async_copy(
            ku_hbm.at[:, pl.ds(pl.multiple_of(tp * wk, 128), wk)], ku, w_sem.at[0]
        ),
        pltpu.make_async_copy(
            vu_hbm.at[:, pl.ds(pl.multiple_of(tp * wv, 128), wv)], vu, w_sem.at[1]
        ),
        pltpu.make_async_copy(ro_hbm, ro, w_sem.at[2]),
        pltpu.make_async_copy(mo_hbm, mo, w_sem.at[3]),
    ]
    for copy in weights:
        copy.start()

    def turn(near, far):
        cn, sn = near[0], near[1]
        co, so = far[0, pl.ds(me, 1), :], far[1, pl.ds(me, 1), :]
        return cn * co - sn * so, sn * co + cn * so

    cos_r, sin_r = turn(near_r, far_r)
    cos_m, sin_m = turn(near_m, far_m)

    def rot(x, cosine, sine, swap):
        return (x.astype(F32) * cosine + dot(x, swap[...]) * sine).astype(BF)

    own_rope = rot(rope_ref[...], cos_m, sin_m, swap_m)
    for t in range(NT):
        span = slice(t * half, (t + 1) * half)
        kvb[me, t, :, 0:KVR] = kv_ref[span, :]
        kvb[me, t, :, KVR:KW] = jnp.concatenate(
            [own_rope[span, :], jnp.zeros((half, KW - KVR - ROPE), BF)], axis=-1
        )

    ii = lax.broadcasted_iota(jnp.int32, (rows, rows), 0)
    jj = lax.broadcasted_iota(jnp.int32, (rows, rows), 1)
    low = ii >= jj
    ones_low = jnp.where(low, 1.0, 0.0).astype(F32)
    dec_own[...] = jnp.zeros_like(dec_own)
    dec_own[0:RL, :] = ld_ref[...]
    ld = dec_own[...]
    c_row = dot_nt(ld, ones_low, lax.Precision.HIGHEST)
    c_col = dot_nt(ones_low, ld, lax.Precision.HIGHEST)
    c_end = c_row[:, rows - 1 : rows]
    dec_own[...] = jnp.broadcast_to(jnp.exp(c_end), dec_own.shape)
    states, keys = [], []
    for h in range(RL):
        key = rot(rk_ref[:, h * QK : (h + 1) * QK], cos_r, sin_r, swap_r)
        keys.append(key)
        tail = jnp.exp(c_row[h : h + 1, rows - 1 : rows] - c_col[:, h : h + 1])
        scaled = (key.astype(F32) * tail).T.astype(BF)
        states.append(dot(scaled, rv_ref[:, h * VD : (h + 1) * VD]).astype(BF))
    for g in range(G):
        h, at = divmod(g * r, QK)
        st_own[g] = states[h][at : at + r, :]

    pl.semaphore_wait(barrier, (NP - 1) + (NF - 1) + (NT - 1))

    for g in range(G):
        to = g * stride

        @pl.when(jnp.logical_and(me != to, me < NP - 1))
        def _():
            remote(dec_own, dec.at[me], d_send.at[g], d_recv.at[me], "sp", to).start()
            remote(st_own.at[g], st_in.at[me], s_send.at[g], s_recv.at[me], "sp", to).start()

    def key_copy(to):
        return remote(
            kvb.at[me, tp], kvb.at[me, tp], k_send.at[to], k_recv.at[me], "sp", to
        )

    @pl.loop(1, NP)
    def _(d):
        @pl.when(me + d < NP)
        def _():
            key_copy(me + d).start()

    for h in range(RL):
        query = rot(rq_ref[:, h * QK : (h + 1) * QK], cos_r, sin_r, swap_r)
        rot_ref[h] = query
        gap = jnp.where(low, c_col[:, h : h + 1] - c_row[h : h + 1, :], 0.0)
        w = jnp.where(low, dot_nt(query, keys[h]) * (QK**-0.5) * jnp.exp(gap), 0.0).astype(BF)
        intra_ref[h] = dot(w, rv_ref[:, h * VD : (h + 1) * VD])
        grow_ref[h] = jnp.broadcast_to(
            jnp.exp(c_col[:, h : h + 1]) * (QK**-0.5), (rows, 128)
        )

    weights[0].wait()
    weights[1].wait()
    mq = mq_ref[...]
    width = NOPE + ROPE
    for h in range(ML):
        nope = mq[:, h * width : h * width + NOPE]
        span = slice(h * rows, (h + 1) * rows)
        q_ref[span, 0:KVR] = dot_nt(nope, ku[:, h * NOPE : (h + 1) * NOPE]).astype(BF)
        turned = rot(mq[:, h * width + NOPE : (h + 1) * width], cos_m, sin_m, swap_m)
        q_ref[span, KVR:KW] = jnp.concatenate(
            [turned, jnp.zeros((rows, KW - KVR - ROPE), BF)], axis=-1
        )

    def scores(at):
        block = kvb[at].reshape(rows, KW)
        return dot_nt(q_ref[...], block) * (width**-0.5), block[:, 0:KVR]

    s, latent = scores(me)
    hide = jnp.where(low, 0.0, -1e30).astype(F32)
    s = s + jnp.concatenate([hide] * ML, axis=0)
    top = jnp.max(s, axis=-1, keepdims=True)
    e = jnp.exp(s - top)
    m_ref[...] = jnp.broadcast_to(top, m_ref.shape)
    l_ref[...] = jnp.broadcast_to(jnp.sum(e, axis=-1, keepdims=True), l_ref.shape)
    acc_ref[...] = dot(e.astype(BF), latent)

    @pl.when(lax.rem(me, stride) == 0)
    def _():
        g = lax.div(me, stride)
        head = lax.div(g * r, QK)
        st_in[me] = st_own[g]
        dec[me] = dec_own[...]

        def scan(n, pre):
            pre_out[n] = pre.astype(BF)

            @pl.when(jnp.logical_and(n > 0, n != me))
            def _():
                remote(pre_out.at[n], pre_in.at[g], h_send.at[n], h_recv.at[g], "sp", n).start()

            @pl.when(jnp.logical_and(n < NP - 1, n != me))
            def _():
                remote(dec_own, dec.at[n], d_send.at[0], d_recv.at[n], "sp", n).wait_recv()
                remote(st_own.at[0], st_in.at[n], s_send.at[0], s_recv.at[n], "sp", n).wait_recv()

            factor = dec[n, pl.ds(head, 1), 0:1]
            return pre * factor + st_in[n].astype(F32)

        last = lax.fori_loop(0, NP - 1, scan, jnp.zeros((r, VD), F32))
        pre_out[NP - 1] = last.astype(BF)

        @pl.when(me != NP - 1)
        def _():
            remote(
                pre_out.at[NP - 1], pre_in.at[g], h_send.at[NP - 1], h_recv.at[g], "sp", NP - 1
            ).start()

        pre_in[g] = pre_out[me]

    def forward(at, k):
        to = lax.rem(tp + k, NT)
        return remote(
            kvb.at[at, tp], kvb.at[at, tp], f_send.at[k, at], f_recv.at[tp, at], "tp", to
        )

    @pl.loop(1, NP + 1)
    def _(d):
        @pl.when(d <= me)
        def _():
            at = me - d
            remote(kvb.at[at, tp], kvb.at[at, tp], k_send.at[at], k_recv.at[at], "sp", at).wait_recv()
            for k in range(1, NT):
                forward(at, k).start()

        @pl.when(jnp.logical_and(d >= 2, d - 1 <= me))
        def _():
            at = me - d + 1
            for k in range(1, NT):
                src = lax.rem(tp + k, NT)
                remote(
                    kvb.at[at, src], kvb.at[at, src], f_send.at[k, at], f_recv.at[src, at], "tp", src
                ).wait_recv()
            s, latent = scores(at)
            before = m_ref[:, 0:1]
            top = jnp.maximum(before, jnp.max(s, axis=-1, keepdims=True))
            e = jnp.exp(s - top)
            shrink = jnp.exp(before - top)
            total = l_ref[:, 0:1] * shrink + jnp.sum(e, axis=-1, keepdims=True)
            m_ref[...] = jnp.broadcast_to(top, m_ref.shape)
            l_ref[...] = jnp.broadcast_to(total, l_ref.shape)
            acc_ref[...] = acc_ref[...] * shrink + dot(e.astype(BF), latent)

    def heads_copy(kind, k):
        to = lax.rem(fs + k, NF)
        return remote(
            gath.at[fs, kind], gath.at[fs, kind], g_send.at[k, kind], g_recv.at[fs, kind], "fs", to
        )

    for h in range(ML):
        span = slice(h * rows, (h + 1) * rows)
        total = l_ref[span, :]
        mean = (acc_ref[span, :] / total[:, 0:1]).astype(BF)
        gath[fs, 1, :, h * VDM : (h + 1) * VDM] = dot(mean, vu[:, h * VDM : (h + 1) * VDM]).astype(BF)
        lw_ref[h : h + 1, :] = (m_ref[span, :] + jnp.log(total)).T[0:1, :]
    for k in range(1, NF):
        heads_copy(1, k).start()

    @pl.when(me > 0)
    def _():
        for g in range(G):
            @pl.when(me != g * stride)
            def _():
                remote(
                    pre_out.at[0], pre_in.at[g], h_send.at[0], h_recv.at[g], "sp", g * stride
                ).wait_recv()

    @pl.when(me == 0)
    def _():
        pre_in[...] = jnp.zeros_like(pre_in)

    per = G // RL
    for h in range(RL):
        state = pre_in[h * per : (h + 1) * per].reshape(QK, VD)
        kept = intra_ref[h] + dot(rot_ref[h], state) * grow_ref[h][:, 0:1]
        normed = kept * lax.rsqrt(jnp.mean(kept * kept, axis=-1, keepdims=True) + 1e-06)
        normed = normed * gain_ref[0:1, h * VD : (h + 1) * VD]
        gath[fs, 0, :, h * VD : (h + 1) * VD] = normed.astype(BF)
    for k in range(1, NF):
        heads_copy(0, k).start()

    weights[2].wait()
    weights[3].wait()

    def partial_copy(s, k):
        to = lax.rem(tp + k, NT)
        return remote(part.at[s, to], tin.at[tp, s], t_send.at[k, s], t_recv.at[tp, s], "tp", to)

    def project(s):
        whole = (dot(gath[s, 1], mo[...]) + dot(gath[s, 0], ro[...])).astype(BF)
        for t in range(NT):
            part[s, t] = whole[t * half : (t + 1) * half, :]
        for k in range(1, NT):
            partial_copy(s, k).start()

    def summed(s):
        total = part[s, tp].astype(F32)
        for k in range(1, NT):
            src = lax.rem(tp + k, NT)
            remote(part.at[s, 0], tin.at[src, s], t_send.at[k, s], t_recv.at[src, s], "tp", src).wait_recv()
            total = total + tin[src, s].astype(F32)
        return total.astype(BF)

    project(fs)
    own = summed(fs)
    cols = out_ref.shape[1] // NF
    for k in range(1, NF):
        s = lax.rem(fs + k, NF)
        for kind in (1, 0):
            remote(
                gath.at[s, kind], gath.at[s, kind], g_send.at[k, kind], g_recv.at[s, kind], "fs", s
            ).wait_recv()
        project(s)

    def back_copy(k):
        s = lax.rem(fs + k, NF)
        return remote(osum.at[s], oin.at[fs], o_send.at[k], o_recv.at[fs], "fs", s)

    for k in range(1, NF):
        s = lax.rem(fs + k, NF)
        osum[s] = summed(s)
        back_copy(k).start()
    out_ref[:, pl.ds(pl.multiple_of(fs * cols, 128), cols)] = own

    for g in range(G):
        @pl.when(jnp.logical_and(me != g * stride, me < NP - 1))
        def _():
            remote(dec_own, dec.at[me], d_send.at[g], d_recv.at[me], "sp", g * stride).wait_send()
            remote(st_own.at[g], st_in.at[me], s_send.at[g], s_recv.at[me], "sp", g * stride).wait_send()

    @pl.loop(1, NP)
    def _(d):
        @pl.when(me + d < NP)
        def _():
            key_copy(me + d).wait_send()

        @pl.when(d <= me)
        def _():
            for k in range(1, NT):
                forward(me - d, k).wait_send()

        @pl.when(jnp.logical_and(lax.rem(me, stride) == 0, d != me))
        def _():
            g = lax.div(me, stride)
            remote(pre_out.at[d], pre_in.at[g], h_send.at[d], h_recv.at[g], "sp", d).wait_send()

    for k in range(1, NF):
        for kind in range(2):
            heads_copy(kind, k).wait_send()
    for s in range(NF):
        for k in range(1, NT):
            partial_copy(s, k).wait_send()
    for k in range(1, NF):
        back_copy(k).wait_send()
    for k in range(1, NF):
        s = lax.rem(fs + k, NF)
        remote(osum.at[s], oin.at[s], o_send.at[k], o_recv.at[s], "fs", s).wait_recv()
        out_ref[:, pl.ds(pl.multiple_of(s * cols, 128), cols)] = oin[s]


def on_device(
    counts,
    ret_query, ret_key, ret_value, log_decay, ret_gain, mla_query,
    kv_latent, rope_key, key_up, value_up, ret_out, mla_out,
):
    NP, NF, NT = counts
    rows = ret_query.shape[0]
    RL = ret_value.shape[2] // VD
    ML = mla_query.shape[2] // (NOPE + ROPE)
    G = min(NP, RL * QK // 16)
    r = RL * QK // G
    half = rows // NT
    cols = ret_out.shape[1]
    near_r, far_r, swap_r = tables(QK // 2, rows, NP)
    near_m, far_m, swap_m = tables(ROPE // 2, rows, NP)
    flat = lambda a: a.reshape(rows, a.shape[2])
    vm = pl.BlockSpec(memory_space=pltpu.VMEM)
    hbm = pl.BlockSpec(memory_space=pl.ANY)
    V = pltpu.VMEM
    D = pltpu.SemaphoreType.DMA
    out, lw = pl.pallas_call(
        functools.partial(kernel, (NP, NF, NT, RL, ML, G)),
        out_shape=(
            jax.ShapeDtypeStruct((half, cols * NF), BF),
            jax.ShapeDtypeStruct((ML, rows), F32),
        ),
        in_specs=[vm] * 14 + [hbm] * 4,
        out_specs=(vm, vm),
        scratch_shapes=[
            V((KVR, ML * NOPE), BF), V((KVR, ML * VDM), BF),
            V(ret_out.shape, BF), V(mla_out.shape, BF),
            V((NP, NT, half, KW), BF), V((ML * rows, KW), BF),
            V((ML * rows, 128), F32), V((ML * rows, 128), F32), V((ML * rows, KVR), F32),
            V((8, 128), F32), V((NP, 8, 128), F32),
            V((G, r, VD), BF), V((NP, r, VD), BF), V((NP, r, VD), BF), V((G, r, VD), BF),
            V((NF, 2, rows, ML * VDM), BF), V((NF, NT, half, cols), BF),
            V((NT, NF, half, cols), BF), V((NF, half, cols), BF), V((NF, half, cols), BF),
            V((RL, rows, VD), F32), V((RL, rows, QK), BF), V((RL, rows, 128), F32),
            D((4,)), D((G,)), D((NP,)), D((G,)), D((NP,)), D((NP,)), D((G,)), D((NP,)), D((NP,)),
            D((NT, NP)), D((NT, NP)), D((NF, 2)), D((NF, 2)), D((NT, NF)), D((NT, NF)),
            D((NF,)), D((NF,)),
        ],
        compiler_params=pltpu.CompilerParams(collective_id=0, has_side_effects=True),
    )(
        flat(ret_query), flat(ret_key), flat(ret_value), log_decay.reshape(RL, rows),
        ret_gain.reshape(1, RL * VD), flat(mla_query), flat(kv_latent), flat(rope_key),
        jnp.asarray(near_r), jnp.asarray(far_r), jnp.asarray(swap_r, BF),
        jnp.asarray(near_m), jnp.asarray(far_m), jnp.asarray(swap_m, BF),
        key_up, value_up, ret_out, mla_out,
    )
    return out.reshape(half, 1, cols * NF), lw.reshape(1, ML, rows)


def solution(mesh):
    counts = tuple(mesh.shape[a] for a in ("sp", "fs", "tp"))
    wide = P("sp", "fs", "tp")
    in_specs = (
        wide, wide, wide, P("fs", "tp", "sp"), P("tp"), wide,
        P("sp", "fs", None), P("sp", "fs", None), P(), P(), P("tp", "fs"), P("tp", "fs"),
    )
    out_specs = (P(("sp", "tp"), "fs", None), P("fs", "tp", "sp"))
    return jax.shard_map(
        functools.partial(on_device, counts),
        mesh=mesh, in_specs=in_specs, out_specs=out_specs, check_vma=False,
    )
```

time: 124 us -> 45.4 us (0.37)
  the two profiles are of different devices: /device:TPU:0 before, /device:TPU:27 now
where the time goes in v1:
time: 45.4 us; the launch traced here: 45.1 us
  Pallas kernels  40.8 us (90%)
  local copies, waits for them, and re-layouts  3.69 us (8%)
  between operations  0.65 us (1%)
    pallas_call x1, Pallas kernels, on_device(): pl.pallas_call(functools.partial(kernel, (NP, NF, NT, RL, ML, G)), out_sh...  40.8 us
    unnamed x5, local copies, waits for them, and re-layouts  3.69 us

profile of v1, /device:TPU:27, one launch (start us, length us, event | category | flops | bytes accessed | tf_op | source)
XLA Modules:
  0.0 45.1 jit_solution(16496969771017247380)
XLA Ops:
  0.6 1.4 %copy.20 = bf16[128,1,64]{2,0,1:T(8,128)(2,1)} copy(bf16[128,1,64]{0,2,1:T(8,128)(2,1)} %param.25) | data formatting | bytes 32768 | tf_op args[7]
  2.1 40.8 %shard_map.185 = (bf16[64,2048]{1,0:T(8,128)(2,1)}, f32[4,128]{1,0:T(4,128)}) custom-call(bf16[128,256]{1,0:T(8,128)(2,1)} %bitcast.14, bf16[128,256]{1,0:T(8,128)(2,1)} %bitcast.15, bf16[128,512]{1,0:T(8,128)(2,1)} %bitcast.13, f32[2,128]{1,0:T(2,128)} %bitcast.19, f32[1,512]{1,0:T(1,128)} %bitcast.17, bf16[128,768]{1,0:T(8,128)(2,1)} %bitcast.11, ...), custom_call_target="tpu_custom_call" | custom-call | tf_op jit(solution)/shard_map/pallas_call | solution.py:400
  42.8 0.0 copy-start
  42.8 1.7 %copy.23 = bf16[64,1,2048]{2,0,1:T(8,128)(2,1)} copy(bf16[64,1,2048]{2,0,1:T(8,128)(2,1)} %bitcast.10) | data formatting | bytes 524288
  44.5 0.0 copy-done
  44.5 0.6 %copy.24 = f32[1,4,128]{2,1,0:T(4,128)} copy(f32[1,4,128]{2,1,0:T(4,128)S(1)} %bitcast.18) | data formatting | bytes 4096
Async XLA Ops:
  42.8 1.7 %copy-start = (f32[4,128]{1,0:T(4,128)S(1)}, f32[4,128]{1,0:T(4,128)}, u32[]{:S(2)}) copy-start(f32[4,128]{1,0:T(4,128)} %get-tuple-element.5) | copy-start | bytes 6148

commit v2 on v1

--- a/solution.py
+++ b/solution.py
@@ -58,16 +58,19 @@
     dec_own, dec, st_own, st_in, pre_out, pre_in,
     gath, part, tin, osum, oin, intra_ref, rot_ref, grow_ref,
     w_sem, d_send, d_recv, s_send, s_recv, h_send, h_recv, k_send, k_recv,
-    f_send, f_recv, g_send, g_recv, t_send, t_recv, o_send, o_recv,
+    f_send, f_recv, y_send, g_send, g_recv, t_send, t_recv, o_send, o_recv,
 ):
     NP, NF, NT, RL, ML, G = sizes
     stride = NP // G
+    NY = max(i for i in range(1, math.isqrt(NP) + 1) if NP % i == 0)
+    NZ = NP // NY
     rows = rq_ref.shape[0]
     half = rows // NT
     r = st_own.shape[1]
     me = lax.axis_index("sp")
     fs = lax.axis_index("fs")
     tp = lax.axis_index("tp")
+    z, y = lax.div(me, NY), lax.rem(me, NY)
 
     def remote(src, dst, ss, rs, axis, to):
         return pltpu.make_async_remote_copy(
@@ -107,7 +110,7 @@
     def rot(x, cosine, sine, swap):
         return (x.astype(F32) * cosine + dot(x, swap[...]) * sine).astype(BF)
 
-    own_rope = rot(rope_ref[...], cos_m, sin_m, swap_m)
+    own_rope = rot(rope_ref[...].astype(F32).T.astype(BF), cos_m, sin_m, swap_m)
     for t in range(NT):
         span = slice(t * half, (t + 1) * half)
         kvb[me, t, :, 0:KVR] = kv_ref[span, :]
@@ -152,11 +155,19 @@
             kvb.at[me, tp], kvb.at[me, tp], k_send.at[to], k_recv.at[me], "sp", to
         )
 
-    @pl.loop(1, NP)
-    def _(d):
-        @pl.when(me + d < NP)
-        def _():
-            key_copy(me + d).start()
+    def key_targets(act):
+        for k in range(1, NY):
+            @pl.when(y + k < NY)
+            def _():
+                act(key_copy(me + k))
+
+        @pl.loop(1, NZ)
+        def _(d):
+            @pl.when(z + d < NZ)
+            def _():
+                act(key_copy(me + d * NY))
+
+    key_targets(lambda copy: copy.start())
 
     for h in range(RL):
         query = rot(rq_ref[:, h * QK : (h + 1) * QK], cos_r, sin_r, swap_r)
@@ -233,47 +244,78 @@
             kvb.at[at, tp], kvb.at[at, tp], f_send.at[k, at], f_recv.at[tp, at], "tp", to
         )
 
-    @pl.loop(1, NP + 1)
-    def _(d):
-        @pl.when(d <= me)
-        def _():
-            at = me - d
-            remote(kvb.at[at, tp], kvb.at[at, tp], k_send.at[at], k_recv.at[at], "sp", at).wait_recv()
-            for k in range(1, NT):
-                forward(at, k).start()
-
-        @pl.when(jnp.logical_and(d >= 2, d - 1 <= me))
-        def _():
-            at = me - d + 1
-            for k in range(1, NT):
-                src = lax.rem(tp + k, NT)
-                remote(
-                    kvb.at[at, src], kvb.at[at, src], f_send.at[k, at], f_recv.at[src, at], "tp", src
-                ).wait_recv()
-            s, latent = scores(at)
-            before = m_ref[:, 0:1]
-            top = jnp.maximum(before, jnp.max(s, axis=-1, keepdims=True))
-            e = jnp.exp(s - top)
-            shrink = jnp.exp(before - top)
-            total = l_ref[:, 0:1] * shrink + jnp.sum(e, axis=-1, keepdims=True)
-            m_ref[...] = jnp.broadcast_to(top, m_ref.shape)
-            l_ref[...] = jnp.broadcast_to(total, l_ref.shape)
-            acc_ref[...] = acc_ref[...] * shrink + dot(e.astype(BF), latent)
+    def relay(at, k):
+        to = z * NY + lax.rem(y + k, NY)
+        return remote(
+            kvb.at[at, tp], kvb.at[at, tp], y_send.at[k, at], k_recv.at[at], "sp", to
+        )
+
+    def landed(at):
+        remote(kvb.at[at, tp], kvb.at[at, tp], k_send.at[at], k_recv.at[at], "sp", at).wait_recv()
+        for k in range(1, NT):
+            forward(at, k).start()
+
+    def paired(at):
+        for k in range(1, NT):
+            src = lax.rem(tp + k, NT)
+            remote(
+                kvb.at[at, src], kvb.at[at, src], f_send.at[k, at], f_recv.at[src, at], "tp", src
+            ).wait_recv()
+
+    def attend(block):
+        s = dot_nt(q_ref[...], block) * (width**-0.5)
+        before = m_ref[:, 0:1]
+        top = jnp.maximum(before, jnp.max(s, axis=-1, keepdims=True))
+        e = jnp.exp(s - top)
+        shrink = jnp.exp(before - top)
+        total = l_ref[:, 0:1] * shrink + jnp.sum(e, axis=-1, keepdims=True)
+        m_ref[...] = jnp.broadcast_to(top, m_ref.shape)
+        l_ref[...] = jnp.broadcast_to(total, l_ref.shape)
+        acc_ref[...] = acc_ref[...] * shrink + dot(e.astype(BF), block[:, 0:KVR])
+
+    def direct(j):
+        @pl.when(j <= z)
+        def _():
+            at = me - j * NY
+            landed(at)
+            for k in range(1, NY):
+                relay(at, k).start()
+
+    direct(1)
+    for k in range(1, NY):
+        @pl.when(y >= k)
+        def _():
+            landed(me - k)
+
+    for k in range(1, NY):
+        @pl.when(y >= k)
+        def _():
+            paired(me - k)
+            attend(kvb[me - k].reshape(rows, KW))
+
+    def line(j):
+        direct(j + 1)
+
+        @pl.when(j <= z)
+        def _():
+            first = (z - j) * NY
+            for k in range(1, NY):
+                landed(first + lax.rem(y + k, NY))
+            for k in range(NY):
+                paired(first + lax.rem(y + k, NY))
+            attend(kvb[pl.ds(first, NY)].reshape(NY * rows, KW))
+
+    split = max(NZ // 2, 1)
+
+    @pl.loop(1, split)
+    def _(j):
+        line(j)
 
     def heads_copy(kind, k):
         to = lax.rem(fs + k, NF)
         return remote(
             gath.at[fs, kind], gath.at[fs, kind], g_send.at[k, kind], g_recv.at[fs, kind], "fs", to
         )
-
-    for h in range(ML):
-        span = slice(h * rows, (h + 1) * rows)
-        total = l_ref[span, :]
-        mean = (acc_ref[span, :] / total[:, 0:1]).astype(BF)
-        gath[fs, 1, :, h * VDM : (h + 1) * VDM] = dot(mean, vu[:, h * VDM : (h + 1) * VDM]).astype(BF)
-        lw_ref[h : h + 1, :] = (m_ref[span, :] + jnp.log(total)).T[0:1, :]
-    for k in range(1, NF):
-        heads_copy(1, k).start()
 
     @pl.when(me > 0)
     def _():
@@ -298,6 +340,19 @@
     for k in range(1, NF):
         heads_copy(0, k).start()
 
+    @pl.loop(split, NZ)
+    def _(j):
+        line(j)
+
+    for h in range(ML):
+        span = slice(h * rows, (h + 1) * rows)
+        total = l_ref[span, :]
+        mean = (acc_ref[span, :] / total[:, 0:1]).astype(BF)
+        gath[fs, 1, :, h * VDM : (h + 1) * VDM] = dot(mean, vu[:, h * VDM : (h + 1) * VDM]).astype(BF)
+        lw_ref[h : h + 1, :] = (m_ref[span, :] + jnp.log(total)).T[0:1, :]
+    for k in range(1, NF):
+        heads_copy(1, k).start()
+
     weights[2].wait()
     weights[3].wait()
 
@@ -325,7 +380,7 @@
     cols = out_ref.shape[1] // NF
     for k in range(1, NF):
         s = lax.rem(fs + k, NF)
-        for kind in (1, 0):
+        for kind in (0, 1):
             remote(
                 gath.at[s, kind], gath.at[s, kind], g_send.at[k, kind], g_recv.at[s, kind], "fs", s
             ).wait_recv()
@@ -341,6 +396,15 @@
         back_copy(k).start()
     out_ref[:, pl.ds(pl.multiple_of(fs * cols, 128), cols)] = own
 
+    key_targets(lambda copy: copy.wait_send())
+
+    @pl.loop(1, NZ)
+    def _(j):
+        @pl.when(j <= z)
+        def _():
+            for k in range(1, NY):
+                relay(me - j * NY, k).wait_send()
+
     for g in range(G):
         @pl.when(jnp.logical_and(me != g * stride, me < NP - 1))
         def _():
@@ -349,10 +413,6 @@
 
     @pl.loop(1, NP)
     def _(d):
-        @pl.when(me + d < NP)
-        def _():
-            key_copy(me + d).wait_send()
-
         @pl.when(d <= me)
         def _():
             for k in range(1, NT):
@@ -388,6 +448,7 @@
     ML = mla_query.shape[2] // (NOPE + ROPE)
     G = min(NP, RL * QK // 16)
     r = RL * QK // G
+    lines = max(i for i in range(1, math.isqrt(NP) + 1) if NP % i == 0)
     half = rows // NT
     cols = ret_out.shape[1]
     near_r, far_r, swap_r = tables(QK // 2, rows, NP)
@@ -416,13 +477,13 @@
             V((NT, NF, half, cols), BF), V((NF, half, cols), BF), V((NF, half, cols), BF),
             V((RL, rows, VD), F32), V((RL, rows, QK), BF), V((RL, rows, 128), F32),
             D((4,)), D((G,)), D((NP,)), D((G,)), D((NP,)), D((NP,)), D((G,)), D((NP,)), D((NP,)),
-            D((NT, NP)), D((NT, NP)), D((NF, 2)), D((NF, 2)), D((NT, NF)), D((NT, NF)),
+            D((NT, NP)), D((NT, NP)), D((lines, NP)), D((NF, 2)), D((NF, 2)), D((NT, NF)), D((NT, NF)),
             D((NF,)), D((NF,)),
         ],
         compiler_params=pltpu.CompilerParams(collective_id=0, has_side_effects=True),
     )(
         flat(ret_query), flat(ret_key), flat(ret_value), log_decay.reshape(RL, rows),
-        ret_gain.reshape(1, RL * VD), flat(mla_query), flat(kv_latent), flat(rope_key),
+        ret_gain.reshape(1, RL * VD), flat(mla_query), flat(kv_latent), flat(rope_key).T,
         jnp.asarray(near_r), jnp.asarray(far_r), jnp.asarray(swap_r, BF),
         jnp.asarray(near_m), jnp.asarray(far_m), jnp.asarray(swap_m, BF),
         key_up, value_up, ret_out, mla_out,

time: 45.4 us -> 40.6 us (0.89)
  Pallas kernels: 40.8 us -> 37.5 us
  local copies, waits for them, and re-layouts: 3.69 us -> 2.25 us
    pallas_call x1, Pallas kernels: 40.8 us -> 37.5 us  [on_device(): pl.pallas_call(functools.partial(kernel, (NP, NF, NT, RL, ML, G)), out_sh...]
    unnamed x5 -> x4, local copies, waits for them, and re-layouts: 3.69 us -> 2.25 us
where the time goes in v2:
time: 40.6 us; the launch traced here: 40.4 us
  Pallas kernels  37.5 us (92%)
  local copies, waits for them, and re-layouts  2.25 us (6%)
  between operations  0.65 us (2%)
    pallas_call x1, Pallas kernels, on_device(): pl.pallas_call(functools.partial(kernel, (NP, NF, NT, RL, ML, G)), out_sh...  37.5 us
    unnamed x4, local copies, waits for them, and re-layouts  2.25 us

profile of v2, /device:TPU:27, one launch (start us, length us, event | category | flops | bytes accessed | tf_op | source)
XLA Modules:
  0.0 40.4 jit_solution(11815135006058665878)
XLA Ops:
  0.6 37.5 %shard_map.185 = (bf16[64,2048]{1,0:T(8,128)(2,1)}, f32[4,128]{1,0:T(4,128)}) custom-call(bf16[128,256]{1,0:T(8,128)(2,1)} %bitcast.15, bf16[128,256]{1,0:T(8,128)(2,1)} %bitcast.16, bf16[128,512]{1,0:T(8,128)(2,1)} %bitcast.14, f32[2,128]{1,0:T(2,128)} %bitcast.21, f32[1,512]{1,0:T(1,128)} %bitcast.19, bf16[128,768]{1,0:T(8,128)(2,1)} %bitcast.13, ...), custom_call_target="tpu_custom_call" | custom-call | tf_op jit(solution)/shard_map/pallas_call | solution.py:461
  38.2 0.0 copy-start
  38.2 1.7 %copy.22 = bf16[64,1,2048]{2,0,1:T(8,128)(2,1)} copy(bf16[64,1,2048]{2,0,1:T(8,128)(2,1)} %bitcast.12) | data formatting | bytes 524288
  39.8 0.0 copy-done
  39.9 0.6 %copy.23 = f32[1,4,128]{2,1,0:T(4,128)} copy(f32[1,4,128]{2,1,0:T(4,128)S(1)} %bitcast.20) | data formatting | bytes 4096
Async XLA Ops:
  38.2 1.7 %copy-start = (f32[4,128]{1,0:T(4,128)S(1)}, f32[4,128]{1,0:T(4,128)}, u32[]{:S(2)}) copy-start(f32[4,128]{1,0:T(4,128)} %get-tuple-element.5) | copy-start | bytes 6148

commit v3 on v2

--- a/solution.py
+++ b/solution.py
@@ -16,6 +16,7 @@
 VDM = 128
 KVR = 256
 KW = 384
+CUTS = 2
 MESH = pl.DeviceIdType.MESH
 BF = jnp.bfloat16
 F32 = jnp.float32
@@ -293,23 +294,35 @@
             paired(me - k)
             attend(kvb[me - k].reshape(rows, KW))
 
+    def line_landed(j):
+        for k in range(1, NY):
+            landed((z - j) * NY + lax.rem(y + k, NY))
+
     def line(j):
         direct(j + 1)
 
         @pl.when(j <= z)
         def _():
             first = (z - j) * NY
-            for k in range(1, NY):
-                landed(first + lax.rem(y + k, NY))
+
+            @pl.when(j < NZ - 1)
+            def _():
+                line_landed(j)
+
             for k in range(NY):
                 paired(first + lax.rem(y + k, NY))
             attend(kvb[pl.ds(first, NY)].reshape(NY * rows, KW))
 
-    split = max(NZ // 2, 1)
+    split = max(NZ - 1, 1)
 
     @pl.loop(1, split)
     def _(j):
         line(j)
+
+    if NZ > 1:
+        @pl.when(z == NZ - 1)
+        def _():
+            line_landed(NZ - 1)
 
     def heads_copy(kind, k):
         to = lax.rem(fs + k, NF)
@@ -356,45 +369,61 @@
     weights[2].wait()
     weights[3].wait()
 
-    def partial_copy(s, k):
+    cols = out_ref.shape[1] // NF
+    piece = cols // CUTS
+
+    def partial_copy(i, k):
         to = lax.rem(tp + k, NT)
-        return remote(part.at[s, to], tin.at[tp, s], t_send.at[k, s], t_recv.at[tp, s], "tp", to)
-
-    def project(s):
-        whole = (dot(gath[s, 1], mo[...]) + dot(gath[s, 0], ro[...])).astype(BF)
-        for t in range(NT):
-            part[s, t] = whole[t * half : (t + 1) * half, :]
-        for k in range(1, NT):
-            partial_copy(s, k).start()
-
-    def summed(s):
-        total = part[s, tp].astype(F32)
+        return remote(part.at[i, to], tin.at[tp, i], t_send.at[k, i], t_recv.at[tp, i], "tp", to)
+
+    def project(s, ready):
+        ready(0)
+        base = dot(gath[s, 0], ro[...])
+        ready(1)
+        for c in range(CUTS):
+            span = slice(c * piece, (c + 1) * piece)
+            whole = (base[:, span] + dot(gath[s, 1], mo[:, span])).astype(BF)
+            for t in range(NT):
+                part[s * CUTS + c, t] = whole[t * half : (t + 1) * half, :]
+            for k in range(1, NT):
+                partial_copy(s * CUTS + c, k).start()
+
+    def summed(i):
+        total = part[i, tp].astype(F32)
         for k in range(1, NT):
             src = lax.rem(tp + k, NT)
-            remote(part.at[s, 0], tin.at[src, s], t_send.at[k, s], t_recv.at[src, s], "tp", src).wait_recv()
-            total = total + tin[src, s].astype(F32)
+            remote(part.at[i, 0], tin.at[src, i], t_send.at[k, i], t_recv.at[src, i], "tp", src).wait_recv()
+            total = total + tin[src, i].astype(F32)
         return total.astype(BF)
 
-    project(fs)
-    own = summed(fs)
-    cols = out_ref.shape[1] // NF
+    def place(s, c):
+        return pl.ds(pl.multiple_of(s * cols + c * piece, 128), piece)
+
+    project(fs, lambda kind: None)
+    for c in range(CUTS):
+        out_ref[:, place(fs, c)] = summed(fs * CUTS + c)
     for k in range(1, NF):
         s = lax.rem(fs + k, NF)
-        for kind in (0, 1):
+
+        def ready(kind):
             remote(
                 gath.at[s, kind], gath.at[s, kind], g_send.at[k, kind], g_recv.at[s, kind], "fs", s
             ).wait_recv()
-        project(s)
-
-    def back_copy(k):
+
+        project(s, ready)
+
+    def back_copy(k, c):
         s = lax.rem(fs + k, NF)
-        return remote(osum.at[s], oin.at[fs], o_send.at[k], o_recv.at[fs], "fs", s)
+        return remote(
+            osum.at[s * CUTS + c], oin.at[fs * CUTS + c],
+            o_send.at[k, c], o_recv.at[fs, c], "fs", s,
+        )
 
     for k in range(1, NF):
         s = lax.rem(fs + k, NF)
-        osum[s] = summed(s)
-        back_copy(k).start()
-    out_ref[:, pl.ds(pl.multiple_of(fs * cols, 128), cols)] = own
+        for c in range(CUTS):
+            osum[s * CUTS + c] = summed(s * CUTS + c)
+            back_copy(k, c).start()
 
     key_targets(lambda copy: copy.wait_send())
 
@@ -426,15 +455,18 @@
     for k in range(1, NF):
         for kind in range(2):
             heads_copy(kind, k).wait_send()
-    for s in range(NF):
+    for i in range(NF * CUTS):
         for k in range(1, NT):
-            partial_copy(s, k).wait_send()
-    for k in range(1, NF):
-        back_copy(k).wait_send()
+            partial_copy(i, k).wait_send()
+    for k in range(1, NF):
+        for c in range(CUTS):
+            back_copy(k, c).wait_send()
     for k in range(1, NF):
         s = lax.rem(fs + k, NF)
-        remote(osum.at[s], oin.at[s], o_send.at[k], o_recv.at[s], "fs", s).wait_recv()
-        out_ref[:, pl.ds(pl.multiple_of(s * cols, 128), cols)] = oin[s]
+        for c in range(CUTS):
+            i = s * CUTS + c
+            remote(osum.at[i], oin.at[i], o_send.at[k, c], o_recv.at[s, c], "fs", s).wait_recv()
+            out_ref[:, place(s, c)] = oin[i]
 
 
 def on_device(
@@ -473,12 +505,13 @@
             V((ML * rows, 128), F32), V((ML * rows, 128), F32), V((ML * rows, KVR), F32),
             V((8, 128), F32), V((NP, 8, 128), F32),
             V((G, r, VD), BF), V((NP, r, VD), BF), V((NP, r, VD), BF), V((G, r, VD), BF),
-            V((NF, 2, rows, ML * VDM), BF), V((NF, NT, half, cols), BF),
-            V((NT, NF, half, cols), BF), V((NF, half, cols), BF), V((NF, half, cols), BF),
+            V((NF, 2, rows, ML * VDM), BF), V((NF * CUTS, NT, half, cols // CUTS), BF),
+            V((NT, NF * CUTS, half, cols // CUTS), BF),
+            V((NF * CUTS, half, cols // CUTS), BF), V((NF * CUTS, half, cols // CUTS), BF),
             V((RL, rows, VD), F32), V((RL, rows, QK), BF), V((RL, rows, 128), F32),
             D((4,)), D((G,)), D((NP,)), D((G,)), D((NP,)), D((NP,)), D((G,)), D((NP,)), D((NP,)),
-            D((NT, NP)), D((NT, NP)), D((lines, NP)), D((NF, 2)), D((NF, 2)), D((NT, NF)), D((NT, NF)),
-            D((NF,)), D((NF,)),
+            D((NT, NP)), D((NT, NP)), D((lines, NP)), D((NF, 2)), D((NF, 2)), D((NT, NF * CUTS)), D((NT, NF * CUTS)),
+            D((NF, CUTS)), D((NF, CUTS)),
         ],
         compiler_params=pltpu.CompilerParams(collective_id=0, has_side_effects=True),
     )(

time: 40.6 us -> 41 us (level); the launches traced: 40.4 us -> 40.3 us
  no operation moved by 1% of the time
where the time goes in v3:
time: 41 us; the launch traced here: 40.3 us
  Pallas kernels  37.4 us (91%)
  local copies, waits for them, and re-layouts  2.25 us (5%)
  between operations  0.65 us (2%)
    pallas_call x1, Pallas kernels, on_device(): pl.pallas_call(functools.partial(kernel, (NP, NF, NT, RL, ML, G)), out_sh...  37.4 us
    unnamed x4, local copies, waits for them, and re-layouts  2.25 us

profile of v3, /device:TPU:27, one launch (start us, length us, event | category | flops | bytes accessed | tf_op | source)
XLA Modules:
  0.0 40.3 jit_solution(8757557315202343465)
XLA Ops:
  0.6 37.4 %shard_map.185 = (bf16[64,2048]{1,0:T(8,128)(2,1)}, f32[4,128]{1,0:T(4,128)}) custom-call(bf16[128,256]{1,0:T(8,128)(2,1)} %bitcast.15, bf16[128,256]{1,0:T(8,128)(2,1)} %bitcast.16, bf16[128,512]{1,0:T(8,128)(2,1)} %bitcast.14, f32[2,128]{1,0:T(2,128)} %bitcast.21, f32[1,512]{1,0:T(1,128)} %bitcast.19, bf16[128,768]{1,0:T(8,128)(2,1)} %bitcast.13, ...), custom_call_target="tpu_custom_call" | custom-call | tf_op jit(solution)/shard_map/pallas_call | solution.py:493
  38.1 0.0 copy-start
  38.1 1.7 %copy.22 = bf16[64,1,2048]{2,0,1:T(8,128)(2,1)} copy(bf16[64,1,2048]{2,0,1:T(8,128)(2,1)} %bitcast.12) | data formatting | bytes 524288
  39.7 0.0 copy-done
  39.7 0.6 %copy.23 = f32[1,4,128]{2,1,0:T(4,128)} copy(f32[1,4,128]{2,1,0:T(4,128)S(1)} %bitcast.20) | data formatting | bytes 4096
Async XLA Ops:
  38.1 1.7 %copy-start = (f32[4,128]{1,0:T(4,128)S(1)}, f32[4,128]{1,0:T(4,128)}, u32[]{:S(2)}) copy-start(f32[4,128]{1,0:T(4,128)} %get-tuple-element.5) | copy-start | bytes 6148

commit v4 on v3

--- a/solution.py
+++ b/solution.py
@@ -305,24 +305,17 @@
         def _():
             first = (z - j) * NY
 
-            @pl.when(j < NZ - 1)
-            def _():
-                line_landed(j)
+            line_landed(j)
 
             for k in range(NY):
                 paired(first + lax.rem(y + k, NY))
             attend(kvb[pl.ds(first, NY)].reshape(NY * rows, KW))
 
-    split = max(NZ - 1, 1)
+    split = max(NZ // 2, 1)
 
     @pl.loop(1, split)
     def _(j):
         line(j)
-
-    if NZ > 1:
-        @pl.when(z == NZ - 1)
-        def _():
-            line_landed(NZ - 1)
 
     def heads_copy(kind, k):
         to = lax.rem(fs + k, NF)

time: 41 us -> 40.4 us (0.985); the launches traced: 40.3 us -> 40.2 us
  no operation moved by 1% of the time
where the time goes in v4:
time: 40.4 us; the launch traced here: 40.2 us
  Pallas kernels  37.3 us (92%)
  local copies, waits for them, and re-layouts  2.25 us (6%)
  between operations  0.65 us (2%)
    pallas_call x1, Pallas kernels, on_device(): pl.pallas_call(functools.partial(kernel, (NP, NF, NT, RL, ML, G)), out_sh...  37.3 us
    unnamed x4, local copies, waits for them, and re-layouts  2.25 us

profile of v4, /device:TPU:27, one launch (start us, length us, event | category | flops | bytes accessed | tf_op | source)
XLA Modules:
  0.0 40.2 jit_solution(1410288901226027925)
XLA Ops:
  0.6 37.3 %shard_map.185 = (bf16[64,2048]{1,0:T(8,128)(2,1)}, f32[4,128]{1,0:T(4,128)}) custom-call(bf16[128,256]{1,0:T(8,128)(2,1)} %bitcast.15, bf16[128,256]{1,0:T(8,128)(2,1)} %bitcast.16, bf16[128,512]{1,0:T(8,128)(2,1)} %bitcast.14, f32[2,128]{1,0:T(2,128)} %bitcast.21, f32[1,512]{1,0:T(1,128)} %bitcast.19, bf16[128,768]{1,0:T(8,128)(2,1)} %bitcast.13, ...), custom_call_target="tpu_custom_call" | custom-call | tf_op jit(solution)/shard_map/pallas_call | solution.py:486
  37.9 0.0 copy-start
  38.0 1.7 %copy.22 = bf16[64,1,2048]{2,0,1:T(8,128)(2,1)} copy(bf16[64,1,2048]{2,0,1:T(8,128)(2,1)} %bitcast.12) | data formatting | bytes 524288
  39.6 0.0 copy-done
  39.6 0.6 %copy.23 = f32[1,4,128]{2,1,0:T(4,128)} copy(f32[1,4,128]{2,1,0:T(4,128)S(1)} %bitcast.20) | data formatting | bytes 4096
Async XLA Ops:
  37.9 1.7 %copy-start = (f32[4,128]{1,0:T(4,128)S(1)}, f32[4,128]{1,0:T(4,128)}, u32[]{:S(2)}) copy-start(f32[4,128]{1,0:T(4,128)} %get-tuple-element.5) | copy-start | bytes 6148
